TPU v7x, 128 devices: a whole 4x4x4 slice. The times are simulated.
128 devices in a mesh: sp: 32 (over z, y, core), tp: 4 (over x).
Axes of the slice: x: 4, y: 4, z: 4, core: 2. Of those that a mesh axis runs over, the one named last changes fastest.
Arguments:
- queries: bfloat16 [24576, 1024], P('sp', 'tp'), may hold values from -6 to 6
- keys: bfloat16 [24576, 1024], P('sp', 'tp'), may hold values from -6 to 6
- values: bfloat16 [24576, 2048], P('sp', 'tp'), may hold values from -6 to 6
- out_gate: bfloat16 [24576, 2048], P('sp', 'tp'), may hold values from -6 to 6
- input_gates: float32 [2, 4, 24576], P(None, 'tp', 'sp'), may hold values from -4 to 300
- forget_gates: float32 [2, 4, 24576], P(None, 'tp', 'sp'), may hold values from -1 to 16
- doc_ids: int32 [24576], P('sp'), may hold values from 0 to 15, never falling along the last dimension, each value on 1 to 3072 neighbouring positions
- head_gain: float32 [2048], P('tp'), may hold values from 0.1 to 1.9
- w_out: bfloat16 [2048, 2048], P('tp'), may hold values from -0.25 to 0.25
- resid: bfloat16 [24576, 2048], P(('sp', 'tp')), may hold values from -30 to 30
- norm_gain: float32 [2048], replicated, may hold values from 0.1 to 1.9
- w_up: bfloat16 [2048, 8192], P('sp', 'tp'), may hold values from -0.125 to 0.125
- w_down: bfloat16 [8192, 2048], P('tp', 'sp'), may hold values from -0.0625 to 0.0625
Outputs:
- layer_out: bfloat16 [24576, 2048], P(('sp', 'tp'))
Inputs may be any that keep to these rules, and one draw needn't show every extreme that they name: `doc_ids`: document numbers never fall along the positions.
All inputs are finite; a program needn't handle non-finite values.
Results may differ from a plain program's by a relative error of at most 0.013.
Values may be sent and summed in bfloat16 or wider, within the bound.
A program may use at most 128 MiB of HBM per device.

v0:
```python
import jax
import jax.numpy as jnp
from jax import lax
from jax.sharding import Mesh
from jax.sharding import PartitionSpec as P

SP = ("sp_0", "sp_1", "sp_2")
SP_TP = ("sp_0", "sp_1", "sp_2", "tp")
eps = 1e-06
far_low = -1e30


def neutral_like(value, identity):
    return jax.tree.map(
        lambda a, e: jnp.broadcast_to(jnp.asarray(e, a.dtype), a.shape), value, identity
    )


def gathered_once(value, axis):
    leaves = jax.tree.leaves(value)
    turns = sorted(range(len(leaves)), key=lambda k: -leaves[k].size)
    width = (1, *leaves[turns[0]].shape)[-1]
    lines = [
        jnp.pad(leaves[k].reshape(-1), (0, -leaves[k].size % width)).reshape(-1, width)
        for k in turns
    ]
    both, at, found = (lax.all_gather(jnp.concatenate(lines), axis), 0, {})
    for k, line in zip(turns, lines):
        section = both[:, at : at + len(line)].reshape(len(both), -1)
        found[k] = section[:, : leaves[k].size].reshape(-1, *leaves[k].shape)
        at += len(line)
    numbers = iter(range(len(leaves)))
    return jax.tree.map(lambda _: found[next(numbers)], value)


def carried_in(value, axes, combine, identity, reverse):
    before = start = neutral_like(value, identity)
    running = value
    for axis in reversed(axes):
        length, index = (lax.axis_size(axis), lax.axis_index(axis))
        pieces = gathered_once(
            jax.tree.map(
                lambda part, kind: part.astype(kind),
                running,
                jax.tree.map(lambda a: jnp.bfloat16 if a.dtype == jnp.float32 else a.dtype, value),
            ),
            axis,
        )
        inside, running = (start, start)
        for k in reversed(range(length)) if reverse else range(length):
            passed = k > index if reverse else k < index
            running = combine(
                running, jax.tree.map(lambda part, own: part[k].astype(own.dtype), pieces, value)
            )
            inside = jax.tree.map(lambda new, old: jnp.where(passed, new, old), running, inside)
        before = combine(inside, before)
    return before


def split_up(value, dim, length):
    dims = value.shape
    pieces = value.reshape(*dims[:dim], length, dims[dim] // length, *dims[dim + 1 :])
    return jnp.moveaxis(pieces, dim, 0)


def sent_and_summed(value, axis, dim):
    length = lax.axis_size(axis)
    pieces = lax.all_to_all(split_up(value, dim, length), axis, 0, 0, tiled=True)
    return jnp.sum(pieces.astype(jnp.float32), axis=0)


def summarize(keys_blk, values_blk, in_gate, forget_pre, doc_pos):
    logf = jax.nn.log_sigmoid(forget_pre)
    cum = jnp.cumsum(logf)
    length = keys_blk.shape[0]
    last_doc = doc_pos[length - 1]
    tail = doc_pos == last_doc
    total = cum[length - 1]
    exponent = jnp.where(tail, total - cum + in_gate, far_low)
    peak = jnp.max(exponent)
    scaled = jnp.exp(exponent - peak)
    weighted = (keys_blk * scaled[:, None]).astype(jnp.bfloat16)
    memory = jnp.einsum("sd,sv->dv", weighted, values_blk, preferred_element_type=jnp.float32)
    norm_keys = jnp.sum(weighted.astype(jnp.float32), axis=0)
    return (memory, norm_keys, peak, total, doc_pos[0], last_doc, jnp.zeros((), jnp.float32))


def emit(queries_blk, keys_blk, values_blk, in_gate, forget_pre, doc_pos, state):
    memory, norm_keys, top_in, total_in, first_in, last_in, empty_in = state
    scale = queries_blk.shape[1] ** (-0.5)
    logf = jax.nn.log_sigmoid(forget_pre)
    cum = jnp.cumsum(logf)
    length = queries_blk.shape[0]
    place = jnp.arange(length)
    keep = (place[:, None] >= place[None, :]) & (doc_pos[:, None] == doc_pos[None, :])
    exponent = jnp.where(keep, cum[:, None] - cum[None, :] + in_gate[None, :], far_low)
    usable = (doc_pos == last_in) & (empty_in < 0.5)
    carried = jnp.where(usable, cum + top_in, far_low)
    peak = jnp.maximum(carried, jnp.max(exponent, axis=1))
    scores = (
        jnp.einsum("td,sd->ts", queries_blk, keys_blk, preferred_element_type=jnp.float32) * scale
    )
    weights = jnp.where(keep, scores * jnp.exp(exponent - peak[:, None]), 0.0)
    inter = jnp.where(usable, jnp.exp(carried - peak), 0.0)
    query_wide = queries_blk.astype(jnp.float32)
    numer = jnp.dot(weights.astype(jnp.bfloat16), values_blk, preferred_element_type=jnp.float32)
    numer = numer + (inter * scale)[:, None] * jnp.dot(query_wide, memory)
    denom = jnp.sum(weights, axis=1) + inter * scale * jnp.dot(query_wide, norm_keys)
    return numer / jnp.maximum(jnp.abs(denom), 1.0)[:, None]


def combine(early, late):
    e_mem, e_keys, e_top, e_total, e_first, e_last, e_empty = early
    l_mem, l_keys, l_top, l_total, l_first, l_last, l_empty = late
    linked = (l_first == e_last) & (l_first == l_last) & (e_empty < 0.5)
    top = jnp.where(linked, jnp.maximum(l_top, e_top + l_total), l_top)
    early_part = jnp.where(linked, jnp.exp(jnp.minimum(e_top + l_total - top, 0.0)), 0.0)
    late_part = jnp.exp(l_top - top)
    joined = (
        early_part * e_mem + late_part * l_mem,
        early_part * e_keys + late_part * l_keys,
        top,
        e_total + l_total,
        jnp.where(e_empty > 0.5, l_first, e_first),
        l_last,
        jnp.zeros_like(l_empty),
    )
    return tuple((jnp.where(l_empty > 0.5, a, b) for a, b in zip(early, joined)))


def direction(queries3, keys3, values3, in_gates, forget_pre, doc_pos, backward):
    if backward:
        queries3, keys3, values3 = (queries3[::-1], keys3[::-1], values3[::-1])
        in_gates, forget_pre, doc_pos = (in_gates[:, ::-1], forget_pre[:, ::-1], doc_pos[::-1])
    summary = jax.vmap(summarize, in_axes=(1, 1, 0, 0, None))(
        keys3, values3, in_gates, forget_pre, doc_pos
    )
    heads = in_gates.shape[0]
    start = (
        jnp.zeros((heads, keys3.shape[2], values3.shape[2]), jnp.float32),
        jnp.zeros((heads, keys3.shape[2]), jnp.float32),
        jnp.full((heads,), far_low, jnp.float32),
        jnp.zeros((heads,), jnp.float32),
        jnp.full((heads,), -1.0, jnp.float32),
        jnp.full((heads,), -1.0, jnp.float32),
        jnp.ones((heads,), jnp.float32),
    )
    if backward:
        incoming = carried_in(summary, SP, jax.vmap(combine), start, True)
    else:
        incoming = carried_in(summary, SP, jax.vmap(combine), start, False)
    result = jax.vmap(emit, in_axes=(1, 1, 1, 0, 0, None, 0), out_axes=1)(
        queries3, keys3, values3, in_gates, forget_pre, doc_pos, incoming
    )
    if backward:
        result = result[::-1]
    return result


def fetch_weights(w_up, w_down):
    up_full = lax.all_gather(w_up, SP, axis=0, tiled=True)
    down_full = lax.all_gather(w_down, SP, axis=1, tiled=True)
    return (up_full, down_full)


def rms_scale(mixed, norm_gain):
    factor = lax.rsqrt(jnp.mean(mixed * mixed, axis=-1, keepdims=True) + eps)
    return (mixed * factor * norm_gain).astype(jnp.bfloat16)


def shards(
    queries,
    keys,
    values,
    out_gate,
    input_gates,
    forget_gates,
    doc_ids,
    head_gain,
    w_out,
    resid,
    norm_gain,
    w_up,
    w_down,
):
    length = queries.shape[0]
    heads = input_gates.shape[1]
    queries3 = queries.reshape(length, heads, -1)
    keys3 = keys.reshape(length, heads, -1)
    values3 = values.reshape(length, heads, -1)
    doc_pos = doc_ids.astype(jnp.float32)
    memory = direction(queries3, keys3, values3, input_gates[0], forget_gates[0], doc_pos, False)
    memory = memory + direction(
        queries3, keys3, values3, input_gates[1], forget_gates[1], doc_pos, True
    )
    normed = memory * lax.rsqrt(jnp.mean(memory * memory, axis=-1, keepdims=True) + eps)
    gate = jax.nn.sigmoid(out_gate.astype(jnp.float32)).reshape(length, heads, -1)
    readout = (
        (normed * head_gain.reshape(heads, -1) * gate).astype(jnp.bfloat16).reshape(length, -1)
    )
    up_full, down_full = fetch_weights(w_up, w_down)
    picked = readout
    mixed = resid.astype(jnp.float32) + sent_and_summed(
        jnp.dot(picked, w_out, preferred_element_type=jnp.float32).astype(jnp.bfloat16), "tp", 0
    )
    scaled = rms_scale(mixed, norm_gain)
    product = jnp.dot(
        lax.all_gather(scaled, "tp", axis=0, tiled=True),
        up_full,
        preferred_element_type=jnp.float32,
    )
    hidden = jnp.square(jax.nn.relu(product)).astype(jnp.bfloat16)
    picked = hidden
    return (
        mixed
        + sent_and_summed(
            jnp.dot(picked, down_full, preferred_element_type=jnp.float32).astype(jnp.bfloat16),
            "tp",
            0,
        )
    ).astype(jnp.bfloat16)


def solution(mesh):
    split = Mesh(mesh.devices.reshape(4, 4, 2, mesh.shape["tp"]), ("sp_0", "sp_1", "sp_2", "tp"))
    return jax.shard_map(
        shards,
        mesh=split,
        in_specs=(
            P(SP, "tp"),
            P(SP, "tp"),
            P(SP, "tp"),
            P(SP, "tp"),
            P(None, "tp", SP),
            P(None, "tp", SP),
            P(SP),
            P("tp"),
            P("tp", None),
            P(SP_TP, None),
            P(),
            P(SP, "tp"),
            P("tp", SP),
        ),
        out_specs=P(SP_TP, None),
        check_vma=False,
    )
```

profile of v0, /device:TPU:0, one launch (start us, length us, event | category | flops | bytes accessed | tf_op | source)
XLA Modules:
  0.0 496.2 jit_solution(1414788614506800733)
XLA Ops:
  6.5 0.9 negate_reduce_fusion
  8.8 0.7 slice.962
  9.4 0.7 convert_element_type.975
  10.7 0.7 slice_reduce_fusion.2
  13.3 2.1 fusion.304
  16.0 0.6 subtract_exponential_fusion
  16.6 1.2 fusion.204
  17.8 1.9 convolution_convert_fusion.3
  20.6 2.2 all-gather.6
  37.3 1.4 concatenate.19
  38.8 3.8 reverse.15
  42.7 11.9 %reverse.16 = bf16[768,512]{1,0:T(8,128)(2,1)} reverse(bf16[768,512]{1,0:T(8,128)(2,1)} %param.15), dimensions={0} | reverse | bytes 1572864 | tf_op jit(solution)/shard_map/reverse.3
  58.3 1.3 fusion.305
  60.2 0.6 exponential_reduce_fusion
  60.9 1.2 fusion.205
  62.0 1.8 convolution_convert_fusion.2
  64.1 2.2 all-gather.9
  80.7 1.4 concatenate.22
  82.2 1.1 fusion.307
  111.6 1.5 fusion.146
  113.1 1.4 concatenate.20
  114.6 1.1 fusion.309
  144.4 1.5 fusion.147
  145.9 1.4 concatenate.23
  147.7 6.3 %reverse.14 = bf16[768,256]{1,0:T(8,128)(2,1)} reverse(bf16[768,256]{1,0:T(8,128)(2,1)} %param.13), dimensions={0} | reverse | bytes 786432 | tf_op jit(solution)/shard_map/reverse
  154.0 2.3 copy.540
  158.0 1.1 fusion.306
  182.1 1.1 fusion.308
  206.5 2.1 fusion.344
  208.6 2.0 fusion.9
  211.5 1.5 fusion.343
  213.0 0.8 fusion.7
  214.2 4.4 fusion.4
  218.5 13.6 %reverse.17 = f32[768,512]{0,1:T(8,128)} reverse(f32[768,512]{0,1:T(8,128)} %fusion.4), dimensions={0} | reverse | bytes 3145728 | tf_op jit(solution)/shard_map/reverse.5
  232.4 4.4 multiply_reduce_fusion.1
  236.8 2.0 convolution_convert_fusion.1
  238.8 42.3 %all_to_all.10 = bf16[4,192,2048]{2,1,0:T(8,128)(2,1)S(1)} all-to-all(bf16[4,192,2048]{2,1,0:T(8,128)(2,1)S(1)} %bitcast.464), channel_id=1, replica_groups=mesh['sp_0'=4,'sp_1'=4,'sp_2'=2,'tp'=4] {'tp'}, dimensions={0} | all-to-all | bytes 6291456 | tf_op jit(solution)/shard_map/all_to_all | solution.py:68
  282.5 0.8 copy-done.2
  283.4 1.1 multiply_convert_fusion.1
  285.1 0.7 all-gather.24.cloned.1.call-update
  285.8 38.8 %all-gather.20.cloned.1.call-done = bf16[768,2048]{1,0:T(8,128)(2,1)} async-done(((bf16[192,2048]{1,0:T(8,128)(2,1)}), bf16[768,2048]{1,0:T(8,128)(2,1)}) %all-gather.20.cloned.1.call-update) | async-done | bytes 3145744 | tf_op jit(solution)/shard_map/all_gather | solution.py:208
  324.7 55.2 %all-gather.22.cloned.1.call-done = bf16[2048,2048]{1,0:T(8,128)(2,1)} async-done(((bf16[64,2048]{1,0:T(8,128)(2,1)}), bf16[2048,2048]{1,0:T(8,128)(2,1)}) %all-gather.22.cloned.1.call-update) | async-done | bytes 8388624 | tf_op jit(solution)/shard_map/all_gather | solution.py:161
  379.9 11.9 %multiply_convert_fusion = bf16[768,2048]{1,0:T(8,128)(2,1)} fusion(bf16[768,2048]{1,0:T(8,128)(2,1)} %all-gather.20.cloned.1.call-done, bf16[2048,2048]{1,0:T(8,128)(2,1)} %all-gather.22.cloned.1.call-done), kind=kOutput, calls=%fused_computation.1 | convolution fusion | flops 6447169536 | bytes 14680064 | tf_op jit(solution)/shard_map/dot_general | solution.py:207
  391.8 42.8 %all-gather.24.cloned.1.call-done = bf16[2048,2048]{0,1:T(8,128)(2,1)} async-done(((bf16[2048,64]{0,1:T(8,128)(2,1)}), bf16[2048,2048]{0,1:T(8,128)(2,1)}) %all-gather.24.cloned.1.call-update) | async-done | bytes 8388624 | tf_op jit(solution)/shard_map/all_gather | solution.py:162
  434.5 10.1 %convolution_convert_fusion = bf16[768,2048]{1,0:T(8,128)(2,1)S(1)} fusion(bf16[768,2048]{1,0:T(8,128)(2,1)} %multiply_convert_fusion, bf16[2048,2048]{0,1:T(8,128)(2,1)} %all-gather.24.cloned.1.call-done), kind=kOutput, calls=%fused_computation.3 | convolution fusion | flops 6444023808 | bytes 14680064 | tf_op jit(solution)/shard_map/dot_general | solution.py:217
  444.6 42.0 %all_to_all.11 = bf16[4,192,2048]{2,1,0:T(8,128)(2,1)S(1)} all-to-all(bf16[4,192,2048]{2,1,0:T(8,128)(2,1)S(1)} %bitcast.465), channel_id=1, replica_groups=mesh['sp_0'=4,'sp_1'=4,'sp_2'=2,'tp'=4] {'tp'}, dimensions={0} | all-to-all | bytes 6291456 | tf_op jit(solution)/shard_map/all_to_all | solution.py:68
  487.3 0.8 copy-done.3
  488.1 1.2 add_convert_fusion
  (216 shorter events, 28.4 us)
Async XLA Ops:
  6.5 230.3 %copy-start = (bf16[512,2048]{1,0:T(8,128)(2,1)S(1)}, bf16[512,2048]{1,0:T(8,128)(2,1)}, u32[]{:S(2)}) copy-start(bf16[512,2048]{1,0:T(8,128)(2,1)} %param.21) | copy-start | bytes 6291460
  6.5 75.6 %all-gather.26.cloned.1.call-start = ((), (), s32[]{:S(2)}) async-start(), calls=%async_computation.5 | async-start | bytes 1351680 | tf_op jit(solution)/shard_map/all_gather | solution.py:27
  17.8 21.0 %copy-start.5 = (bf16[768,256]{1,0:T(8,128)(2,1)S(1)}, bf16[768,256]{1,0:T(8,128)(2,1)}, u32[]{:S(2)}) copy-start(bf16[768,256]{1,0:T(8,128)(2,1)} %param.14) | copy-start | bytes 1179652
  38.7 75.9 %all-gather.30.cloned.1.call-start = ((), (), s32[]{:S(2)}) async-start(), calls=%async_computation.7 | async-start | bytes 1351680 | tf_op jit(solution)/shard_map/all_gather | solution.py:27
  82.1 75.9 %all-gather.28.cloned.1.call-start = ((), (), s32[]{:S(2)}) async-start(), calls=%async_computation.6 | async-start | bytes 1351680 | tf_op jit(solution)/shard_map/all_gather | solution.py:27
  114.5 67.6 %all-gather.32.cloned.1.call-start = ((), (), s32[]{:S(2)}) async-start(), calls=%async_computation.8 | async-start | bytes 1351680 | tf_op jit(solution)/shard_map/all_gather | solution.py:27
  145.9 60.5 %copy-start.12 = (s32[768]{0:T(1024)S(1)}, s32[768]{0:T(1024)}, u32[]{:S(2)}) copy-start(s32[768]{0:T(1024)} %param.19) | copy-start | bytes 9220
  147.3 177.3 %all-gather.20.cloned.1.call-start = ((), (), s32[]{:S(2)}) async-start(), calls=%async_computation.2 | async-start | bytes 3932160 | tf_op jit(solution)/shard_map/all_gather | solution.py:208
  206.5 2.1 copy-start.9
  208.6 2.9 copy-start.7
  208.6 2.9 copy-start.8
  211.5 1.5 copy-start.10
  218.5 13.6 %copy-start.6 = (bf16[768,256]{1,0:T(8,128)(2,1)S(1)}, bf16[768,256]{1,0:T(8,128)(2,1)}, u32[]{:S(2)}) copy-start(bf16[768,256]{1,0:T(8,128)(2,1)} %param.13) | copy-start | bytes 1179652
  232.4 4.4 copy-start.11
  232.4 4.4 copy-start.14
  281.1 1.1 copy-start.4
  282.2 1.1 copy-start.2
  282.2 1.1 copy-start.13
  284.5 95.4 %all-gather.22.cloned.1.call-start = ((), (), s32[]{:S(2)}) async-start(), calls=%async_computation.3 | async-start | bytes 8650752 | tf_op jit(solution)/shard_map/all_gather | solution.py:161
  285.1 149.5 %all-gather.24.cloned.1.call-start = ((), (), s32[]{:S(2)}) async-start(), calls=%async_computation.4 | async-start | bytes 8650752 | tf_op jit(solution)/shard_map/all_gather | solution.py:162
  486.7 1.4 copy-start.3
  486.7 2.6 copy-start.1
Sparse Core Ops, SparseCore 0:
  38.8 26.7 all-gather.25
  82.2 26.6 all-gather.29
  114.6 26.8 all-gather.27
  147.5 26.8 all-gather.31
  284.6 39.9 all-gather.19
  326.8 53.0 all-gather.21
  382.1 52.3 all-gather.23
where the time goes:
time: 502 us; the launch traced here: 496 us
  waiting for transfers between devices  138 us (27%)
  between operations  134 us (27%)
  blocking collectives  88.7 us (18%)
  local copies, waits for them, and re-layouts  72.9 us (15%)
  matrix products  43.3 us (9%)
  other arithmetic  18.8 us (4%)
    all_to_all x2, blocking collectives, sent_and_summed(): lax.all_to_all(split_up(value, dim, length), axis, 0, 0, tiled=True)  84.3 us
    all_gather x1, waiting for transfers between devices, fetch_weights(): up_full = lax.all_gather(w_up, SP, axis=0, tiled=True)  55.2 us
    all_gather x1, waiting for transfers between devices, fetch_weights(): down_full = lax.all_gather(w_down, SP, axis=1, tiled=True)  42.8 us
    all_gather x1, waiting for transfers between devices, shards(): lax.all_gather(scaled, 'tp', axis=0, tiled=True)  38.8 us
    another operation x7, local copies, waits for them, and re-layouts  35.8 us
    slice x30, local copies, waits for them, and re-layouts, carried_in(): part[k].astype(own.dtype)  17.1 us
    dot_general x1, matrix products, shards(): jnp.dot(lax.all_gather(scaled, 'tp', axis=0, tiled=True), up_full, prefer...  11.9 us
    dot_general x1, matrix products, shards(): jnp.dot(picked, down_full, preferred_element_type=jnp.float32)  10.1 us
  transfers between devices with their start and end apart: 7, of which 3 were waited for; matrix products, arithmetic and copies ran while one was open for 14% of the time, Pallas kernels for 0%

commit v1 on v0

--- a/solution.py
+++ b/solution.py
@@ -8,6 +8,12 @@
 SP_TP = ("sp_0", "sp_1", "sp_2", "tp")
 eps = 1e-06
 far_low = -1e30
+
+
+def gather_by_exchange(x, axis, dim):
+    size = lax.axis_size(axis)
+    repeats = [size if d == dim else 1 for d in range(x.ndim)]
+    return lax.all_to_all(jnp.tile(x, repeats), axis, split_axis=dim, concat_axis=dim, tiled=True)
 
 
 def neutral_like(value, identity):
@@ -205,9 +211,7 @@
     )
     scaled = rms_scale(mixed, norm_gain)
     product = jnp.dot(
-        lax.all_gather(scaled, "tp", axis=0, tiled=True),
-        up_full,
-        preferred_element_type=jnp.float32,
+        gather_by_exchange(scaled, "tp", 0), up_full, preferred_element_type=jnp.float32
     )
     hidden = jnp.square(jax.nn.relu(product)).astype(jnp.bfloat16)
     picked = hidden

time: 502 us -> 405 us (0.81)
  waiting for transfers between devices: 138 us -> 1.2 us
  blocking collectives: 88.7 us -> 125 us
    all_gather x1, waiting for transfers between devices: 55.2 us -> 0.01 us  [fetch_weights(): up_full = lax.all_gather(w_up, SP, axis=0, tiled=True)]
    all_gather x1, waiting for transfers between devices: 42.8 us -> 0.01 us  [fetch_weights(): down_full = lax.all_gather(w_down, SP, axis=1, tiled=True)]
    all_to_all x0 -> x1, blocking collectives: none -> 40.1 us  [gather_by_exchange(): lax.all_to_all(jnp.tile(x, repeats), axis, split_axis=dim, concat_axis=di...]
    all_gather x1 -> x0, waiting for transfers between devices: 38.8 us -> none  [shards(): lax.all_gather(scaled, 'tp', axis=0, tiled=True)]
    another operation x7 -> x8, local copies, waits for them, and re-layouts: 35.8 us -> 36.4 us
  transfers between devices with their start and end apart: 7 -> 6, of which waited for: 3 -> 0; matrix products, arithmetic and copies ran while one was open for 14% -> 27% of each run, Pallas kernels for 0% -> 0%
where the time goes in v1:
time: 405 us; the launch traced here: 398 us
  between operations  136 us (34%)
  blocking collectives  125 us (31%)
  local copies, waits for them, and re-layouts  74.3 us (18%)
  matrix products  44.2 us (11%)
  other arithmetic  17.6 us (4%)
    all_to_all x2, blocking collectives, sent_and_summed(): lax.all_to_all(split_up(value, dim, length), axis, 0, 0, tiled=True)  80.6 us
    all_to_all x1, blocking collectives, gather_by_exchange(): lax.all_to_all(jnp.tile(x, repeats), axis, split_axis=dim, concat_axis=di...  40.1 us
    another operation x7, local copies, waits for them, and re-layouts  36 us
    slice x30, local copies, waits for them, and re-layouts, carried_in(): part[k].astype(own.dtype)  17.4 us
    dot_general x1, matrix products, shards(): jnp.dot(gather_by_exchange(scaled, 'tp', 0), up_full, preferred_element_t...  11.9 us
    dot_general x1, matrix products, shards(): jnp.dot(picked, down_full, preferred_element_type=jnp.float32)  10.1 us
  transfers between devices with their start and end apart: 6, of which 0 were waited for; matrix products, arithmetic and copies ran while one was open for 27% of the time, Pallas kernels for 0%

profile of v1, /device:TPU:0, one launch (start us, length us, event | category | flops | bytes accessed | tf_op | source)
XLA Modules:
  0.0 398.1 jit_solution(3723046107489536877)
XLA Ops:
  6.5 0.9 negate_reduce_fusion
  8.8 0.7 slice.962
  9.4 0.7 convert_element_type.975
  10.7 0.7 slice_reduce_fusion.2
  13.3 2.0 fusion.304
  16.5 1.2 fusion.204
  17.6 1.9 convolution_convert_fusion.3
  20.3 2.2 all-gather.6
  37.1 1.4 concatenate.19
  38.6 3.8 reverse.15
  42.5 11.9 %reverse.16 = bf16[768,512]{1,0:T(8,128)(2,1)} reverse(bf16[768,512]{1,0:T(8,128)(2,1)} %param.15), dimensions={0} | reverse | bytes 1572864 | tf_op jit(solution)/shard_map/reverse.3
  58.0 1.2 fusion.305
  60.3 1.2 fusion.205
  61.5 1.8 convolution_convert_fusion.2
  63.5 2.2 all-gather.9
  80.7 1.4 concatenate.22
  82.2 1.3 fusion.307
  87.1 0.6 fusion.317
  94.0 0.6 fusion.318
  112.2 1.5 fusion.146
  113.7 1.4 concatenate.20
  115.2 1.1 fusion.309
  145.3 1.5 fusion.147
  146.8 1.4 concatenate.23
  149.5 6.5 %reverse.14 = bf16[768,256]{1,0:T(8,128)(2,1)} reverse(bf16[768,256]{1,0:T(8,128)(2,1)} %param.13), dimensions={0} | reverse | bytes 786432 | tf_op jit(solution)/shard_map/reverse
  156.0 2.3 copy.540
  159.0 0.6 select_reduce_fusion
  160.0 1.1 fusion.306
  161.1 0.6 fusion.316
  184.3 1.1 fusion.308
  186.8 0.6 fusion.323
  210.2 1.3 convolution_reduce_fusion
  211.5 2.1 fusion.343
  213.6 0.8 fusion.7
  214.6 4.3 %fusion.4 = f32[768,512]{0,1:T(8,128)} fusion(f32[768,512]{0,1:T(8,128)S(1)} %fusion.7, bf16[768,256]{1,0:T(8,128)(2,1)S(1)} %copy-done.9, f32[768]{0:T(1024)S(1)} %get-tuple-element.16, f32[768]{0:T(1024)S(1)} %get-tuple-element.17, bf16[4,262,512]{2,1,0:T(8,128)(2,1)} %all-gather.29.cloned.1.call-done, f32[]{:T(128)} %bitcast.267, f32[]{:T(128)} %bitcast.266, ...), kind=kOutput, calls=%fused_computation.16 | convolution fusion | flops 210632704 | bytes 6190592 | tf_op jit(solution)/shard_map/vmap()/dot_general | solution.py:113
  218.9 13.6 %reverse.17 = f32[768,512]{0,1:T(8,128)} reverse(f32[768,512]{0,1:T(8,128)} %fusion.4), dimensions={0} | reverse | bytes 3145728 | tf_op jit(solution)/shard_map/reverse.5
  232.5 1.3 convolution_reduce_fusion.1
  233.8 2.6 fusion.344
  236.5 0.8 fusion.9
  237.9 3.4 multiply_reduce_fusion.1
  241.4 2.0 convolution_convert_fusion.1
  243.3 42.1 %all_to_all.19 = bf16[4,192,2048]{2,1,0:T(8,128)(2,1)S(1)} all-to-all(bf16[4,192,2048]{2,1,0:T(8,128)(2,1)S(1)} %bitcast.466), channel_id=1, replica_groups=mesh['sp_0'=4,'sp_1'=4,'sp_2'=2,'tp'=4] {'tp'}, dimensions={0} | all-to-all | bytes 6291456 | tf_op jit(solution)/shard_map/all_to_all | solution.py:74
  288.2 40.1 %all_to_all.20 = bf16[4,192,2048]{2,1,0:T(8,128)(2,1)} all-to-all(bf16[4,192,2048]{2,1,0:T(8,128)(2,1)S(1)} %tile.2), channel_id=1, replica_groups=mesh['sp_0'=4,'sp_1'=4,'sp_2'=2,'tp'=4] {'tp'}, dimensions={0} | all-to-all | bytes 6291456 | tf_op jit(solution)/shard_map/all_to_all | solution.py:16
  328.2 11.9 %multiply_convert_fusion = bf16[768,2048]{1,0:T(8,128)(2,1)} fusion(bf16[768,2048]{1,0:T(8,128)(2,1)} %bitcast.465, bf16[2048,2048]{1,0:T(8,128)(2,1)} %all-gather.19.cloned.1.call-done), kind=kOutput, calls=%fused_computation.1 | convolution fusion | flops 6447169536 | bytes 14680064 | tf_op jit(solution)/shard_map/dot_general | solution.py:213
  340.1 10.1 %convolution_convert_fusion = bf16[768,2048]{1,0:T(8,128)(2,1)S(1)} fusion(bf16[768,2048]{1,0:T(8,128)(2,1)} %multiply_convert_fusion, bf16[2048,2048]{0,1:T(8,128)(2,1)} %all-gather.21.cloned.1.call-done), kind=kOutput, calls=%fused_computation.3 | convolution fusion | flops 6444023808 | bytes 14680064 | tf_op jit(solution)/shard_map/dot_general | solution.py:221
  350.2 38.4 %all_to_all.21 = bf16[4,192,2048]{2,1,0:T(8,128)(2,1)S(1)} all-to-all(bf16[4,192,2048]{2,1,0:T(8,128)(2,1)S(1)} %bitcast.467), channel_id=1, replica_groups=mesh['sp_0'=4,'sp_1'=4,'sp_2'=2,'tp'=4] {'tp'}, dimensions={0} | all-to-all | bytes 6291456 | tf_op jit(solution)/shard_map/all_to_all | solution.py:74
  389.2 0.8 copy-done.3
  390.0 1.2 add_convert_fusion
  (217 shorter events, 28.4 us)
Async XLA Ops:
  6.5 234.8 %copy-start = (bf16[512,2048]{1,0:T(8,128)(2,1)S(1)}, bf16[512,2048]{1,0:T(8,128)(2,1)}, u32[]{:S(2)}) copy-start(bf16[512,2048]{1,0:T(8,128)(2,1)} %param.21) | copy-start | bytes 6291460
  6.5 75.6 %all-gather.23.cloned.1.call-start = ((), (), s32[]{:S(2)}) async-start(), calls=%async_computation.5 | async-start | bytes 1351680 | tf_op jit(solution)/shard_map/all_gather | solution.py:33
  17.6 21.0 %copy-start.6 = (bf16[768,256]{1,0:T(8,128)(2,1)S(1)}, bf16[768,256]{1,0:T(8,128)(2,1)}, u32[]{:S(2)}) copy-start(bf16[768,256]{1,0:T(8,128)(2,1)} %param.14) | copy-start | bytes 1179652
  38.5 76.7 %all-gather.27.cloned.1.call-start = ((), (), s32[]{:S(2)}) async-start(), calls=%async_computation.7 | async-start | bytes 1351680 | tf_op jit(solution)/shard_map/all_gather | solution.py:33
  82.1 77.9 %all-gather.25.cloned.1.call-start = ((), (), s32[]{:S(2)}) async-start(), calls=%async_computation.6 | async-start | bytes 1351680 | tf_op jit(solution)/shard_map/all_gather | solution.py:33
  115.1 69.2 %all-gather.29.cloned.1.call-start = ((), (), s32[]{:S(2)}) async-start(), calls=%async_computation.8 | async-start | bytes 1351680 | tf_op jit(solution)/shard_map/all_gather | solution.py:33
  148.2 180.0 %all-gather.19.cloned.1.call-start = ((), (), s32[]{:S(2)}) async-start(), calls=%async_computation.3 | async-start | bytes 8650752 | tf_op jit(solution)/shard_map/all_gather | solution.py:167
  148.8 191.3 %all-gather.21.cloned.1.call-start = ((), (), s32[]{:S(2)}) async-start(), calls=%async_computation.4 | async-start | bytes 8650752 | tf_op jit(solution)/shard_map/all_gather | solution.py:168
  211.5 2.1 copy-start.11
  213.6 1.0 copy-start.9
  218.9 14.9 %copy-start.13 = (s32[768]{0:T(1024)S(1)}, s32[768]{0:T(1024)}, u32[]{:S(2)}) copy-start(s32[768]{0:T(1024)} %param.19) | copy-start | bytes 9220
  218.9 14.9 %copy-start.7 = (bf16[768,256]{1,0:T(8,128)(2,1)S(1)}, bf16[768,256]{1,0:T(8,128)(2,1)}, u32[]{:S(2)}) copy-start(bf16[768,256]{1,0:T(8,128)(2,1)} %param.14) | copy-start | bytes 1179652
  233.8 2.6 copy-start.10
  236.5 1.4 copy-start.5
  236.5 1.5 copy-start.8
  237.9 3.4 copy-start.12
  237.9 3.4 copy-start.15
  285.5 1.1 copy-start.4
  286.6 1.1 copy-start.2
  286.6 0.7 copy-start.14
  388.6 1.4 copy-start.3
  388.6 2.6 copy-start.1
Sparse Core Ops, SparseCore 0:
  38.6 26.7 all-gather.22
  82.2 26.6 all-gather.26
  115.2 26.8 all-gather.24
  148.3 26.8 all-gather.28
  177.3 53.1 all-gather.18
  232.6 52.3 all-gather.20
